TPU v7x, 256 devices: a whole 4x4x8 slice. The times are simulated.
256 devices in a mesh: ep: 16 (over y, x), tp: 16 (over z, core).
Axes of the slice: x: 4, y: 4, z: 8, core: 2. Of those that a mesh axis runs over, the one named last changes fastest.
Arguments:
- mix_tokens: bfloat16 [4096, 4096], P('ep'), may hold values from -6 to 6
- mix_gain: float32 [4096], replicated, may hold values from 0.1 to 1.9
- value_weight: bfloat16 [4096, 2048], P(None, 'tp'), may hold values from -0.09375 to 0.09375
- inner_weight: bfloat16 [4096, 2048], P(None, 'tp'), may hold values from -0.09375 to 0.09375
- outer_weight: bfloat16 [4096, 2048], P(None, 'tp'), may hold values from -0.09375 to 0.09375
- conv_taps: float32 [3, 2048], P(None, 'tp'), may hold values from -3 to 3
- mix_weight: bfloat16 [2048, 4096], P('tp'), may hold values from -0.125 to 0.125
- moe_tokens: bfloat16 [4096, 4096], P('ep'), may hold values from -6 to 6
- moe_gain: float32 [4096], replicated, may hold values from 0.1 to 1.9
- router_group: bfloat16 [4096, 4], replicated, may hold values from -0.09375 to 0.09375
- router_expert: bfloat16 [4096, 16], replicated, may hold values from -0.09375 to 0.09375
- expert_routes: int32 [4096, 2], P('ep'), may hold values from 0 to 15, as said below
- gate_weight: bfloat16 [16, 4096, 2048], P('ep', None, 'tp'), may hold values from -0.09375 to 0.09375
- up_weight: bfloat16 [16, 4096, 2048], P('ep', None, 'tp'), may hold values from -0.09375 to 0.09375
- down_weight: bfloat16 [16, 2048, 4096], P('ep', 'tp'), may hold values from -0.5 to 0.5
Outputs:
- mixer_out: bfloat16 [4096, 4096], P(('ep', 'tp'))
- expert_out: bfloat16 [4096, 4096], P(('ep', 'tp'))
Inputs may be any that keep to these rules, and one draw needn't show every extreme that they name: `expert_routes`: the two experts of a row are different and lie in one group of 4 consecutive expert numbers. In each aligned block of 16 rows no expert is named more than 4 times, and in every draw some experts are named exactly 4 times in every block.
All inputs are finite; a program needn't handle non-finite values.
Results may differ from a plain program's by a relative error of at most 0.0076.
Values may be sent and summed in bfloat16 or wider, within the bound.
No kernel may reach another device: no remote copies, remote signals or barrier semaphores. Data moves between devices by JAX's collectives and lax.ppermute only.
A program may use at most 128 MiB of HBM per device.

v0:
```python
import jax
import jax.numpy as jnp
from jax import lax
from jax.sharding import PartitionSpec as P

TAPS = 3
EXPERTS = 16
GROUPS = 4
TOPK = 2
MOE_SHARE = 16
EPG = 4
CAP = 4


def from_behind(value, axis, steps):
    count = lax.axis_size(axis)
    initial, last = (max(0, -steps), min(count, count - steps))
    return lax.ppermute(value, axis, [(source, source + steps) for source in range(initial, last)])


def rms_rows(inputs, gain_vec):
    values = inputs.astype(jnp.float32)
    inverse = lax.rsqrt(jnp.mean(values * values, axis=-1, keepdims=True) + 1e-06)
    return (values * inverse * gain_vec).astype(jnp.bfloat16)


def route_weights(normed, routes, router_group, router_expert):
    group_logit = jnp.dot(normed, router_group, preferred_element_type=jnp.float32)
    expert_logit = jnp.dot(normed, router_expert, preferred_element_type=jnp.float32)
    group_exp = jnp.exp(group_logit)
    group_id = routes[:, 0] // EPG
    group_pick = (group_id[:, None] == jnp.arange(GROUPS, dtype=jnp.int32)[None, :]).astype(
        jnp.float32
    )
    group_gate = jnp.sum(group_exp * group_pick, axis=1) / jnp.sum(group_exp, axis=1)
    expert_pick = (
        routes[:, :, None] == jnp.arange(EXPERTS, dtype=jnp.int32)[None, None, :]
    ).astype(jnp.float32)
    chosen = jnp.exp(jnp.sum(expert_logit[:, None, :] * expert_pick, axis=2))
    return group_gate[:, None] * chosen / jnp.sum(chosen, axis=1, keepdims=True)


def block_ranks(routes):
    blocks = routes.shape[0]
    entries = routes.reshape(blocks, MOE_SHARE * TOPK)
    one_hot = (entries[:, :, None] == jnp.arange(EXPERTS, dtype=jnp.int32)[None, None, :]).astype(
        jnp.int32
    )
    before = jnp.cumsum(one_hot, axis=1) - one_hot
    return jnp.sum(before * one_hot, axis=2).reshape(routes.shape)


def dispatch_rows(normed, routes):
    slot_ids = routes * CAP + block_ranks(routes)
    targets = jnp.arange(EXPERTS * CAP, dtype=jnp.int32)
    select = (slot_ids[:, None, :, :] == targets[None, :, None, None]).astype(jnp.int32)
    select = jnp.sum(select, axis=3).astype(jnp.bfloat16)
    placed = jnp.einsum("bcs,bsd->bcd", select, normed, preferred_element_type=jnp.float32)
    return placed.astype(jnp.bfloat16).reshape(normed.shape[0], EXPERTS, CAP, normed.shape[2])


def expert_hidden(arrived, gate_weight, up_weight):
    gate_proj = jnp.einsum(
        "besd,edf->besf", arrived, gate_weight, preferred_element_type=jnp.float32
    )
    up_proj = jnp.einsum("besd,edf->besf", arrived, up_weight, preferred_element_type=jnp.float32)
    return (jax.nn.silu(gate_proj) * up_proj).astype(jnp.bfloat16)


def mixer_half(
    mix_tokens, mix_gain, value_weight, inner_weight, outer_weight, conv_taps, mix_weight
):
    normed = rms_rows(mix_tokens, mix_gain)
    value_proj = jnp.dot(normed, value_weight, preferred_element_type=jnp.float32)
    inner_proj = jnp.dot(normed, inner_weight, preferred_element_type=jnp.float32)
    outer_proj = jnp.dot(normed, outer_weight, preferred_element_type=jnp.float32)
    gated_in = (inner_proj * value_proj).astype(jnp.bfloat16)
    earlier = from_behind(gated_in[gated_in.shape[0] - (TAPS - 1) :], "ep", 1)
    padded = jnp.concatenate([earlier, gated_in], axis=0).astype(jnp.float32)
    seq_rows = gated_in.shape[0]
    mixed_conv = conv_taps[0] * padded[0:seq_rows]
    for tap_index in range(1, TAPS):
        mixed_conv = mixed_conv + conv_taps[tap_index] * padded[tap_index : tap_index + seq_rows]
    conv_out = (outer_proj * mixed_conv).astype(jnp.bfloat16)
    summed = lax.psum_scatter(
        jnp.dot(conv_out, mix_weight, preferred_element_type=jnp.float32),
        "tp",
        scatter_dimension=0,
        tiled=True,
    )
    return summed.astype(jnp.bfloat16)


def local(
    mix_tokens,
    mix_gain,
    value_weight,
    inner_weight,
    outer_weight,
    conv_taps,
    mix_weight,
    moe_tokens,
    moe_gain,
    router_group,
    router_expert,
    expert_routes,
    gate_weight,
    up_weight,
    down_weight,
):
    mixer_out = mixer_half(
        mix_tokens, mix_gain, value_weight, inner_weight, outer_weight, conv_taps, mix_weight
    )
    tp_index = lax.axis_index("tp")
    model_width = moe_tokens.shape[1]
    own_routes = lax.dynamic_slice_in_dim(expert_routes, tp_index * MOE_SHARE, MOE_SHARE, 0)
    own_tokens = lax.dynamic_slice_in_dim(moe_tokens, tp_index * MOE_SHARE, MOE_SHARE, 0)
    own_normed = rms_rows(own_tokens, moe_gain)
    placed = dispatch_rows(own_normed[None], own_routes[None])[0]
    arrived = lax.all_to_all(placed, "ep", split_axis=0, concat_axis=1, tiled=True)
    hidden = expert_hidden(
        lax.all_gather(arrived[None], "tp", axis=0, tiled=True), gate_weight, up_weight
    )
    local_experts = hidden.shape[1]
    slot_count = hidden.shape[2]
    per_block = local_experts * slot_count
    partial_value = jnp.einsum(
        "besf,efd->besd", hidden, down_weight, preferred_element_type=jnp.float32
    )
    summed = lax.psum_scatter(
        partial_value.reshape(per_block * lax.axis_size("tp"), model_width),
        "tp",
        scatter_dimension=0,
        tiled=True,
    )
    results = summed.astype(jnp.bfloat16).reshape(
        local_experts, slot_count // CAP, CAP, model_width
    )
    returned = lax.all_to_all(results, "ep", split_axis=1, concat_axis=0, tiled=True).reshape(
        EXPERTS * CAP, model_width
    )
    weights = route_weights(own_normed, own_routes, router_group, router_expert)
    own_slots = own_routes * CAP + block_ranks(own_routes[None])[0]
    picked = jnp.take(returned, own_slots, axis=0).astype(jnp.float32)
    expert_out = jnp.sum(weights[:, :, None] * picked, axis=1).astype(jnp.bfloat16)
    return (mixer_out, expert_out)


def solution(mesh):
    return jax.shard_map(
        local,
        mesh=mesh,
        in_specs=(
            P("ep", None),
            P(),
            P(None, "tp"),
            P(None, "tp"),
            P(None, "tp"),
            P(None, "tp"),
            P("tp", None),
            P("ep", None),
            P(),
            P(),
            P(),
            P("ep", None),
            P("ep", None, "tp"),
            P("ep", None, "tp"),
            P("ep", "tp", None),
        ),
        out_specs=(P(("ep", "tp"), None), P(("ep", "tp"), None)),
        check_vma=False,
    )
```

profile of v0, /device:TPU:2, one launch (start us, length us, event | category | flops | bytes accessed | tf_op | source)
XLA Modules:
  0.0 281.7 jit_solution(8360812834643250856)
XLA Ops:
  7.2 0.8 constant_dynamic-slice_fusion
  8.4 0.2 select_reduce_fusion
  8.7 0.8 compare_and_fusion
  9.6 1.0 fusion.37
  10.6 1.3 convolution_convert_fusion
  11.9 0.2 squeeze_reshape.7
  12.1 17.4 %all_to_all.8 = bf16[16,4,4096]{2,1,0:T(4,128)(2,1)S(1)} all-to-all(bf16[16,4,4096]{2,1,0:T(4,128)(2,1)S(1)} %squeeze_reshape.7), channel_id=1, replica_groups=mesh['ep'=16,'tp'=16] {'ep'}, dimensions={0} | all-to-all | bytes 1048576 | tf_op jit(solution)/shard_map/all_to_all | solution.py:120
  29.5 0.9 broadcast_in_dim.12
  30.5 55.9 %all-gather.2.cloned.1.call-done = bf16[16,1,64,4096]{3,2,1,0:T(8,128)(2,1)} async-done(((bf16[1,1,64,4096]{3,2,1,0:T(8,128)(2,1)}), bf16[16,1,64,4096]{3,2,1,0:T(8,128)(2,1)}) %all-gather.2.cloned.1.call-update) | async-done | bytes 8388624 | tf_op jit(solution)/shard_map/all_gather | solution.py:122
  86.5 5.9 %fusion.7 = f32[16,1,64,128]{3,2,0,1:T(8,128)S(1)} fusion(bf16[16,1,64,4096]{3,2,1,0:T(8,128)(2,1)} %all-gather.2.cloned.1.call-done, bf16[1,4096,128]{2,1,0:T(8,128)(2,1)} %param.27), kind=kOutput, calls=%fused_computation.11 | convolution fusion | flops 1073741824 | bytes 9961472 | tf_op jit(solution)/shard_map/besd,edf->besf/dot_general | solution.py:63
  92.4 14.4 %fusion.23 = f32[16,64,4096]{2,1,0:T(8,128)} fusion(bf16[16,1,64,4096]{3,2,1,0:T(8,128)(2,1)} %all-gather.2.cloned.1.call-done, bf16[1,128,4096]{2,1,0:T(8,128)(2,1)S(1)} %copy-done, bf16[1,4096,128]{2,1,0:T(8,128)(2,1)S(1)} %copy-done.2, f32[16,1,64,128]{3,2,0,1:T(8,128)S(1)} %fusion.7), kind=kOutput, calls=%fused_computation.16 | convolution fusion | flops 2148270080 | bytes 27787264 | tf_op jit(solution)/shard_map/besf,efd->besd/dot_general | solution.py:127
  106.9 1.5 copy-done.1
  108.4 0.5 fusion.4
  108.9 2.1 fusion.57
  111.0 0.9 fusion.26
  111.9 3.4 %collective-permute-start = (bf16[2,128]{1,0:T(2,128)(2,1)S(1)}, bf16[2,128]{1,0:T(2,128)(2,1)S(1)}, u32[]{:S(2)}, u32[]{:S(2)}) collective-permute-start(bf16[2,128]{1,0:T(2,128)(2,1)S(1)} %slice.34), channel_id=1, source_target_pairs={{0,16},{16,32},{32,48},{48,64},{64,80},{80,96},{96,112},{112,128},... | collective-permute-start | bytes 1544 | tf_op jit(solution)/shard_map/ppermute | solution.py:18
  115.3 2.1 collective-permute-done
  117.4 5.0 %fusion.27 = f32[256,4096]{1,0:T(8,128)} fusion(bf16[128,4096]{1,0:T(8,128)(2,1)} %param.21, bf16[4096,128]{1,0:T(8,128)(2,1)} %param.19, f32[258,128]{1,0:T(8,128)S(1)} %maximum_convert_fusion, f32[128]{0:T(128)S(1)} %get-tuple-element.7, f32[128]{0:T(128)S(1)} %get-tuple-element.8, f32[128]{0:T(128)S(1)} %get-tuple-element.6, ...), kind=kOutput, calls=%fused_computation.21 | convolution fusion | flops 541294592 | bytes 8800768 | tf_op jit(solution)/shard_map/dot_general | solution.py:86
  122.4 0.7 copy-done.4
  123.1 1.2 fusion.61
  124.3 1.1 fusion.53
  125.5 80.6 %reduce-scatter.5.cloned.1.call-done = f32[64,4096]{1,0:T(8,128)} async-done(((f32[1024,4096]{1,0:T(8,128)}), f32[64,4096]{1,0:T(8,128)}) %reduce-scatter.5.cloned.1.call-update) | async-done | bytes 1048592 | tf_op jit(solution)/shard_map/reduce_scatter | solution.py:130
  206.1 1.3 convert_element_type.92
  207.4 1.0 reshape.229
  208.4 7.3 %all-to-all-start.1 = ((bf16[1,16,4,4096]{3,2,0,1:T(4,128)(2,1)}), bf16[1,16,4,4096]{3,2,0,1:T(4,128)(2,1)S(1)}, u32[]{:S(2)}, u32[]{:S(2)}) async-start(bf16[1,16,4,4096]{3,2,0,1:T(4,128)(2,1)} %reshape.229), calls=%async_computation.3 | async-start | bytes 1048576 | tf_op jit(solution)/shard_map/all_to_all | solution.py:139
  215.6 0.2 select_reduce_fusion.1
  216.2 54.8 %reduce-scatter.3.cloned.1.call-done = f32[16,4096]{1,0:T(8,128)} async-done(((f32[256,4096]{1,0:T(8,128)}), f32[16,4096]{1,0:T(8,128)}) %reduce-scatter.3.cloned.1.call-update) | async-done | bytes 262160 | tf_op jit(solution)/shard_map/reduce_scatter | solution.py:85
  271.0 1.6 convert_element_type.84
  272.7 0.1 reshape.230
  272.8 0.7 gather_fusion
  273.5 0.2 reshape.232
  273.7 1.5 multiply_reduce_fusion
  (45 shorter events, 1.3 us)
Async XLA Ops:
  7.2 85.2 %copy-start = (bf16[1,128,4096]{2,1,0:T(8,128)(2,1)S(1)}, bf16[1,128,4096]{2,1,0:T(8,128)(2,1)}, u32[]{:S(2)}) copy-start(bf16[1,128,4096]{2,1,0:T(8,128)(2,1)} %param.29) | copy-start | bytes 3145732
  7.2 79.3 %all-gather.2.cloned.1.call-start = ((), (), s32[]{:S(2)}) async-start(), calls=%async_computation.5 | async-start | bytes 8912896 | tf_op jit(solution)/shard_map/all_gather | solution.py:122
  30.5 61.9 %copy-start.2 = (bf16[1,4096,128]{2,1,0:T(8,128)(2,1)S(1)}, bf16[1,4096,128]{2,1,0:T(8,128)(2,1)}, u32[]{:S(2)}) copy-start(bf16[1,4096,128]{2,1,0:T(8,128)(2,1)} %param.28) | copy-start | bytes 3145732
  30.5 175.6 %reduce-scatter.5.cloned.1.call-start = ((), (), s32[]{:S(2)}) async-start(), calls=%async_computation.6 | async-start | bytes 17825792 | tf_op jit(solution)/shard_map/reduce_scatter | solution.py:130
  106.8 1.6 copy-start.1
  106.8 2.1 copy-start.3
  106.8 164.2 %reduce-scatter.3.cloned.1.call-start = ((), (), s32[]{:S(2)}) async-start(), calls=%async_computation.4 | async-start | bytes 4456448 | tf_op jit(solution)/shard_map/reduce_scatter | solution.py:85
  108.4 2.6 copy-start.6
  108.9 6.4 %copy-start.5 = (f32[3,128]{1,0:T(4,128)S(1)}, f32[3,128]{1,0:T(4,128)}, u32[]{:S(2)}) copy-start(f32[3,128]{1,0:T(4,128)} %param.20) | copy-start | bytes 4612
  111.9 5.5 %collective-permute-start = (bf16[2,128]{1,0:T(2,128)(2,1)S(1)}, bf16[2,128]{1,0:T(2,128)(2,1)S(1)}, u32[]{:S(2)}, u32[]{:S(2)}) collective-permute-start(bf16[2,128]{1,0:T(2,128)(2,1)S(1)} %slice.34), channel_id=1, source_target_pairs={{0,16},{16,32},{32,48},{48,64},{64,80},{80,96},{96,112},{112,128},... | collective-permute-start | bytes 1544 | tf_op jit(solution)/shard_map/ppermute | solution.py:18
  122.4 0.7 copy-start.4
  122.4 0.8 copy-start.8
  122.4 1.9 copy-start.7
  208.4 64.3 %all-to-all-start.1 = ((bf16[1,16,4,4096]{3,2,0,1:T(4,128)(2,1)}), bf16[1,16,4,4096]{3,2,0,1:T(4,128)(2,1)S(1)}, u32[]{:S(2)}, u32[]{:S(2)}) async-start(bf16[1,16,4,4096]{3,2,0,1:T(4,128)(2,1)} %reshape.229), calls=%async_computation.3 | async-start | bytes 1048576 | tf_op jit(solution)/shard_map/all_to_all | solution.py:139
Sparse Core Ops, SparseCore 0:
  30.6 55.8 all-gather.1
  107.0 99.0 reduce-scatter.4
  208.6 62.3 reduce-scatter.2
where the time goes:
time: 282 us
  waiting for transfers between devices  193 us (68%)
  matrix products  31.8 us (11%)
  blocking collectives  17.4 us (6%)
  between operations  14 us (5%)
  starting transfers between devices  10.8 us (4%)
  other arithmetic  7.33 us (3%)
  local copies, waits for them, and re-layouts  6.92 us (2%)
    reduce_scatter x1, waiting for transfers between devices, local(): lax.psum_scatter(partial_value.reshape(per_block * lax.axis_size('tp'), m...  80.6 us
    all_gather x1, waiting for transfers between devices, local(): lax.all_gather(arrived[None], 'tp', axis=0, tiled=True)  55.9 us
    reduce_scatter x1, waiting for transfers between devices, mixer_half(): lax.psum_scatter(jnp.dot(conv_out, mix_weight, preferred_element_type=jnp...  54.8 us
    all_to_all x1, blocking collectives, local(): lax.all_to_all(placed, 'ep', split_axis=0, concat_axis=1, tiled=True)  17.4 us
    dot_general x1, matrix products, local(): jnp.einsum('besf,efd->besd', hidden, down_weight, preferred_element_type=...  14.4 us
    all_to_all x1, starting transfers between devices, local(): lax.all_to_all(results, 'ep', split_axis=1, concat_axis=0, tiled=True)  7.27 us
    dot_general x1, matrix products, expert_hidden(): jnp.einsum('besd,edf->besf', arrived, gate_weight, preferred_element_type...  5.93 us
  transfers between devices with their start and end apart: 5, of which 4 were waited for; matrix products, arithmetic and copies ran while one was open for 5% of the time, Pallas kernels for 0%

commit v1 on v0

--- a/solution.py
+++ b/solution.py
@@ -10,6 +10,27 @@
 MOE_SHARE = 16
 EPG = 4
 CAP = 4
+
+
+def joined_along(blocks, dim):
+    blocks = jnp.moveaxis(blocks, 0, dim)
+    dims = blocks.shape
+    return blocks.reshape(*dims[:dim], dims[dim] * dims[dim + 1], *dims[dim + 2 :])
+
+
+def grow_blocks(value, axis):
+    size, here = (lax.axis_size(axis), lax.axis_index(axis))
+    blocks, bit = (value[None], 1)
+    while bit < size:
+        other = lax.ppermute(blocks, axis, [(i, i ^ bit) for i in range(size)])
+        low = here & bit == 0
+        blocks = jnp.concatenate([jnp.where(low, blocks, other), jnp.where(low, other, blocks)])
+        bit *= 2
+    return blocks
+
+
+def gather_by_bits(x, axis, dim):
+    return joined_along(grow_blocks(x, axis), dim)
 
 
 def from_behind(value, axis, steps):
@@ -118,9 +139,7 @@
     own_normed = rms_rows(own_tokens, moe_gain)
     placed = dispatch_rows(own_normed[None], own_routes[None])[0]
     arrived = lax.all_to_all(placed, "ep", split_axis=0, concat_axis=1, tiled=True)
-    hidden = expert_hidden(
-        lax.all_gather(arrived[None], "tp", axis=0, tiled=True), gate_weight, up_weight
-    )
+    hidden = expert_hidden(gather_by_bits(arrived[None], "tp", 0), gate_weight, up_weight)
     local_experts = hidden.shape[1]
     slot_count = hidden.shape[2]
     per_block = local_experts * slot_count

time: 282 us -> 542 us (1.92)
  waiting for transfers between devices: 193 us -> 433 us
  starting transfers between devices: 10.8 us -> 21.2 us
  other arithmetic: 7.33 us -> 16.9 us
    ppermute x0 -> x4, waiting for transfers between devices: none -> 297 us  [grow_blocks(): other = lax.ppermute(blocks, axis, [(i, i ^ bit) for i in range(size)])]
    all_gather x1 -> x0, waiting for transfers between devices: 55.9 us -> none  [local(): lax.all_gather(arrived[None], 'tp', axis=0, tiled=True)]
    ppermute x0 -> x4, starting transfers between devices: none -> 11.5 us  [grow_blocks(): other = lax.ppermute(blocks, axis, [(i, i ^ bit) for i in range(size)])]
    select_n x0 -> x4, other arithmetic: none -> 5.75 us  [grow_blocks(): jnp.where(low, blocks, other)]
  transfers between devices with their start and end apart: 5 -> 8, of which waited for: 4 -> 7; matrix products, arithmetic and copies ran while one was open for 5% -> 3% of each run, Pallas kernels for 0% -> 0%
where the time goes in v1:
time: 542 us
  waiting for transfers between devices  433 us (80%)
  matrix products  28.2 us (5%)
  starting transfers between devices  21.2 us (4%)
  blocking collectives  17.4 us (3%)
  other arithmetic  16.9 us (3%)
  between operations  14.4 us (3%)
  local copies, waits for them, and re-layouts  10.5 us (2%)
    ppermute x4, waiting for transfers between devices, grow_blocks(): other = lax.ppermute(blocks, axis, [(i, i ^ bit) for i in range(size)])  297 us
    reduce_scatter x1, waiting for transfers between devices, local(): lax.psum_scatter(partial_value.reshape(per_block * lax.axis_size('tp'), m...  78.3 us
    reduce_scatter x1, waiting for transfers between devices, mixer_half(): lax.psum_scatter(jnp.dot(conv_out, mix_weight, preferred_element_type=jnp...  54.6 us
    all_to_all x1, blocking collectives, local(): lax.all_to_all(placed, 'ep', split_axis=0, concat_axis=1, tiled=True)  17.4 us
    dot_general x1, matrix products, local(): jnp.einsum('besf,efd->besd', hidden, down_weight, preferred_element_type=...  14.4 us
    ppermute x4, starting transfers between devices, grow_blocks(): other = lax.ppermute(blocks, axis, [(i, i ^ bit) for i in range(size)])  11.5 us
  transfers between devices with their start and end apart: 8, of which 7 were waited for; matrix products, arithmetic and copies ran while one was open for 3% of the time, Pallas kernels for 0%

profile of v1, /device:TPU:2, one launch (start us, length us, event | category | flops | bytes accessed | tf_op | source)
XLA Modules:
  0.0 541.7 jit_solution(15432439459084749076)
XLA Ops:
  9.6 1.0 fusion.14
  10.6 1.3 convolution_convert_fusion
  12.1 17.4 %all_to_all.8 = bf16[16,4,4096]{2,1,0:T(4,128)(2,1)S(1)} all-to-all(bf16[16,4,4096]{2,1,0:T(4,128)(2,1)S(1)} %squeeze_reshape.7), channel_id=1, replica_groups=mesh['ep'=16,'tp'=16] {'ep'}, dimensions={0} | all-to-all | bytes 1048576 | tf_op jit(solution)/shard_map/all_to_all | solution.py:141
  29.8 1.9 collective-permute-done.1
  31.8 1.1 pad_maximum_fusion.2
  32.8 1.9 collective-permute-start.2
  34.7 23.7 %collective-permute-done.2 = bf16[2,1,1,64,4096]{4,3,0,2,1:T(8,128)(2,1)S(1)} collective-permute-done((bf16[2,1,1,64,4096]{4,3,0,2,1:T(8,128)(2,1)}, bf16[2,1,1,64,4096]{4,3,0,2,1:T(8,128)(2,1)S(1)}, u32[]{:S(2)}, u32[]{:S(2)}) %collective-permute-start.2) | collective-permute-done | bytes 1048608 | tf_op jit(solution)/shard_map/ppermute | solution.py:25
  59.9 3.3 collective-permute-start.3
  63.1 90.3 %collective-permute-done.3 = bf16[4,1,1,64,4096]{4,3,0,2,1:T(8,128)(2,1)} collective-permute-done((bf16[4,1,1,64,4096]{4,3,0,2,1:T(8,128)(2,1)S(1)}, bf16[4,1,1,64,4096]{4,3,0,2,1:T(8,128)(2,1)}, u32[]{:S(2)}, u32[]{:S(2)}) %collective-permute-start.3) | collective-permute-done | bytes 2097184 | tf_op jit(solution)/shard_map/ppermute | solution.py:25
  153.4 2.4 broadcast_select_fusion.3
  155.9 2.6 pad_maximum_fusion
  158.5 6.2 %collective-permute-start.4 = (bf16[8,1,1,64,4096]{4,3,0,2,1:T(8,128)(2,1)}, bf16[8,1,1,64,4096]{4,3,0,2,1:T(8,128)(2,1)}, u32[]{:S(2)}, u32[]{:S(2)}) collective-permute-start(bf16[8,1,1,64,4096]{4,3,0,2,1:T(8,128)(2,1)} %pad_maximum_fusion), channel_id=1, source_target_pairs={{0,8},{1,9},{2,10},{3,11},{4,12},{5,13},{6,14},{7,15},{8,0},{9,1},... | collective-permute-start | bytes 12582920 | tf_op jit(solution)/shard_map/ppermute | solution.py:25
  164.7 181.3 %collective-permute-done.4 = bf16[8,1,1,64,4096]{4,3,0,2,1:T(8,128)(2,1)} collective-permute-done((bf16[8,1,1,64,4096]{4,3,0,2,1:T(8,128)(2,1)}, bf16[8,1,1,64,4096]{4,3,0,2,1:T(8,128)(2,1)}, u32[]{:S(2)}, u32[]{:S(2)}) %collective-permute-start.4) | collective-permute-done | bytes 4194336 | tf_op jit(solution)/shard_map/ppermute | solution.py:25
  346.0 3.1 broadcast_select_fusion.1
  349.1 1.9 copy-done.3
  351.1 1.2 copy-done.4
  352.3 2.5 fusion.5
  354.9 14.4 %fusion.10 = f32[16,64,4096]{2,1,0:T(8,128)} fusion(bf16[1,128,4096]{2,1,0:T(8,128)(2,1)S(1)} %copy-done, f32[16,1,64,128]{3,2,0,1:T(8,128)S(1)} %fusion.5, bf16[8,1,1,64,4096]{4,3,0,2,1:T(8,128)(2,1)} %copy-done.4, bf16[8,1,1,64,4096]{4,3,0,2,1:T(8,128)(2,1)} %copy-done.3, bf16[1,4096,128]{2,1,0:T(8,128)(2,1)S(1)} %copy-done.9), kind=kOutput, calls=%fused_computation.25 | convolution fusion | flops 2152464384 | bytes 27787264 | tf_op jit(solution)/shard_map/besf,efd->besd/dot_general | solution.py:146
  369.4 1.5 copy-done.7
  371.4 2.1 fusion.41
  374.4 2.3 collective-permute-start
  376.8 3.1 collective-permute-done
  379.9 4.6 fusion.9
  385.3 1.2 fusion.45
  386.5 1.2 fusion.37
  387.7 78.3 %reduce-scatter.5.cloned.1.call-done = f32[64,4096]{1,0:T(8,128)} async-done(((f32[1024,4096]{1,0:T(8,128)}), f32[64,4096]{1,0:T(8,128)}) %reduce-scatter.5.cloned.1.call-update) | async-done | bytes 1048592 | tf_op jit(solution)/shard_map/reduce_scatter | solution.py:149
  466.0 1.3 convert_element_type.92
  467.3 1.0 reshape.232
  468.3 7.3 %all-to-all-start.1 = ((bf16[1,16,4,4096]{3,2,0,1:T(4,128)(2,1)}), bf16[1,16,4,4096]{3,2,0,1:T(4,128)(2,1)S(1)}, u32[]{:S(2)}, u32[]{:S(2)}) async-start(bf16[1,16,4,4096]{3,2,0,1:T(4,128)(2,1)} %reshape.232), calls=%async_computation.3 | async-start | bytes 1048576 | tf_op jit(solution)/shard_map/all_to_all | solution.py:158
  476.1 54.6 %reduce-scatter.3.cloned.1.call-done = f32[16,4096]{1,0:T(8,128)} async-done(((f32[256,4096]{1,0:T(8,128)}), f32[16,4096]{1,0:T(8,128)}) %reduce-scatter.3.cloned.1.call-update) | async-done | bytes 262160 | tf_op jit(solution)/shard_map/reduce_scatter | solution.py:106
  530.7 1.6 convert_element_type.84
  533.4 1.5 multiply_reduce_fusion
  (73 shorter events, 8.2 us)
Async XLA Ops:
  7.2 347.7 %copy-start = (bf16[1,128,4096]{2,1,0:T(8,128)(2,1)S(1)}, bf16[1,128,4096]{2,1,0:T(8,128)(2,1)}, u32[]{:S(2)}) copy-start(bf16[1,128,4096]{2,1,0:T(8,128)(2,1)} %param.29) | copy-start | bytes 3145732
  7.2 458.8 %reduce-scatter.5.cloned.1.call-start = ((), (), s32[]{:S(2)}) async-start(), calls=%async_computation.5 | async-start | bytes 17825792 | tf_op jit(solution)/shard_map/reduce_scatter | solution.py:149
  29.7 2.0 collective-permute-start.1
  32.8 25.6 %collective-permute-start.2 = (bf16[2,1,1,64,4096]{4,3,0,2,1:T(8,128)(2,1)}, bf16[2,1,1,64,4096]{4,3,0,2,1:T(8,128)(2,1)S(1)}, u32[]{:S(2)}, u32[]{:S(2)}) collective-permute-start(bf16[2,1,1,64,4096]{4,3,0,2,1:T(8,128)(2,1)} %pad_maximum_fusion.2), channel_id=1, source_target_pairs={{0,2},{1,3},{2,0},{3,1},{4,6},{5,7},{6,4},{7,5},{8,10},{9,11},{10,... | collective-permute-start | bytes 3145736 | tf_op jit(solution)/shard_map/ppermute | solution.py:25
  58.5 1.0 copy-start.5
  58.6 1.3 copy-start.6
  59.9 93.6 %collective-permute-start.3 = (bf16[4,1,1,64,4096]{4,3,0,2,1:T(8,128)(2,1)S(1)}, bf16[4,1,1,64,4096]{4,3,0,2,1:T(8,128)(2,1)}, u32[]{:S(2)}, u32[]{:S(2)}) collective-permute-start(bf16[4,1,1,64,4096]{4,3,0,2,1:T(8,128)(2,1)S(1)} %pad_maximum_fusion.1), channel_id=1, source_target_pairs={{0,4},{1,5},{2,6},{3,7},{4,0},{5,1},{6,2},{7,3},{8,12},{9,13},{10,... | collective-permute-start | bytes 6291464 | tf_op jit(solution)/shard_map/ppermute | solution.py:25
  155.9 2.6 copy-start.2
  158.5 187.5 %collective-permute-start.4 = (bf16[8,1,1,64,4096]{4,3,0,2,1:T(8,128)(2,1)}, bf16[8,1,1,64,4096]{4,3,0,2,1:T(8,128)(2,1)}, u32[]{:S(2)}, u32[]{:S(2)}) collective-permute-start(bf16[8,1,1,64,4096]{4,3,0,2,1:T(8,128)(2,1)} %pad_maximum_fusion), channel_id=1, source_target_pairs={{0,8},{1,9},{2,10},{3,11},{4,12},{5,13},{6,14},{7,15},{8,0},{9,1},... | collective-permute-start | bytes 12582920 | tf_op jit(solution)/shard_map/ppermute | solution.py:25
  164.7 187.6 %copy-start.13 = (bf16[1,4096,128]{2,1,0:T(8,128)(2,1)S(1)}, bf16[1,4096,128]{2,1,0:T(8,128)(2,1)}, u32[]{:S(2)}) copy-start(bf16[1,4096,128]{2,1,0:T(8,128)(2,1)} %param.27) | copy-start | bytes 3145732
  349.1 2.0 copy-start.3
  349.1 3.2 copy-start.4
  352.3 2.6 copy-start.9
  369.3 1.6 copy-start.7
  369.3 2.1 copy-start.10
  369.3 161.4 %reduce-scatter.3.cloned.1.call-start = ((), (), s32[]{:S(2)}) async-start(), calls=%async_computation.4 | async-start | bytes 4456448 | tf_op jit(solution)/shard_map/reduce_scatter | solution.py:106
  370.9 2.7 copy-start.14
  371.4 5.4 copy-start.12
  371.4 8.5 %copy-start.8 = (bf16[128,4096]{1,0:T(8,128)(2,1)S(1)}, bf16[128,4096]{1,0:T(8,128)(2,1)}, u32[]{:S(2)}) copy-start(bf16[128,4096]{1,0:T(8,128)(2,1)} %param.21) | copy-start | bytes 3145732
  374.4 5.5 %collective-permute-start = (bf16[2,128]{1,0:T(2,128)(2,1)S(1)}, bf16[2,128]{1,0:T(2,128)(2,1)S(1)}, u32[]{:S(2)}, u32[]{:S(2)}) collective-permute-start(bf16[2,128]{1,0:T(2,128)(2,1)S(1)} %slice.34), channel_id=1, source_target_pairs={{0,16},{16,32},{32,48},{48,64},{64,80},{80,96},{96,112},{112,128},... | collective-permute-start | bytes 1544 | tf_op jit(solution)/shard_map/ppermute | solution.py:39
  384.5 0.7 copy-start.11
  384.6 0.8 copy-start.16
  384.6 1.9 copy-start.15
  386.5 148.4 %copy-start.1 = (bf16[1,128,4096]{2,1,0:T(8,128)(2,1)S(1)}, bf16[1,128,4096]{2,1,0:T(8,128)(2,1)}, u32[]{:S(2)}) copy-start(bf16[1,128,4096]{2,1,0:T(8,128)(2,1)} %param.29) | copy-start | bytes 3145732
  468.3 64.1 %all-to-all-start.1 = ((bf16[1,16,4,4096]{3,2,0,1:T(4,128)(2,1)}), bf16[1,16,4,4096]{3,2,0,1:T(4,128)(2,1)S(1)}, u32[]{:S(2)}, u32[]{:S(2)}) async-start(bf16[1,16,4,4096]{3,2,0,1:T(4,128)(2,1)} %reshape.232), calls=%async_computation.3 | async-start | bytes 1048576 | tf_op jit(solution)/shard_map/all_to_all | solution.py:158
Sparse Core Ops, SparseCore 0:
  369.4 96.5 reduce-scatter.4
  468.6 62.1 reduce-scatter.2
